TPU v7x, 32 devices: a whole 2x2x4 slice. The times are simulated.
32 devices in a mesh: fs: 8 (over z, y), tp: 4 (over x, core).
Axes of the slice: x: 2, y: 2, z: 4, core: 2. Of those that a mesh axis runs over, the one named last changes fastest.
Arguments:
- tokens: bfloat16 [4096, 2048], P(('fs', 'tp')), may hold values from -6 to 6
- routes: int32 [4096, 4], P(('fs', 'tp')), may hold values from 0 to 31, all different within a row; in each aligned block of 128 rows (0 to 127, 128 to 255, ...) at most 24 rows name the same one
- route_weight: float32 [4096, 4], P(('fs', 'tp')), may hold values from 0.1 to 1
- norm_gain: float32 [2048], P('fs'), may hold values from 0.5 to 4
- gate_weight: float32 [32, 2048, 512], P(None, 'fs', 'tp'), may hold values from -0.125 to 0.125
- up_weight: float32 [32, 2048, 512], P(None, 'fs', 'tp'), may hold values from -0.125 to 0.125
- down_weight: float32 [32, 512, 2048], P(None, 'fs', 'tp'), may hold values from -0.0625 to 0.0625
Outputs:
- gate_new: bfloat16 [32, 2048, 512], P(('fs', 'tp'))
- up_new: bfloat16 [32, 2048, 512], P(('fs', 'tp'))
- down_new: bfloat16 [32, 512, 2048], P(('fs', 'tp'))
- mixed: bfloat16 [4096, 2048], P(('fs', 'tp'))
Inputs may be any that keep to these rules, and one draw needn't show every extreme that they name: `routes`: each row names 4 different experts, and every expert is named by some row; within the 128 rows of one device no expert is named by more than 24 rows, and in some blocks an expert is named by exactly 24 rows.
All inputs are finite; a program needn't handle non-finite values.
Results may differ from a plain program's by a relative error of at most 0.0084.
Values may be sent and summed in bfloat16 or wider, within the bound.
A program may use at most 128 MiB of HBM per device.

v0:
```python
import functools

import jax
import jax.numpy as jnp
from jax import lax
from jax.experimental import pallas as pl
from jax.experimental.pallas import tpu as pltpu
from jax.sharding import PartitionSpec as P

norm_epsilon = 1e-06
clamp_limit = 7.0
sigmoid_slope = 1.702
MESH = pl.DeviceIdType.MESH


def feed(inputs, gate_mat, up_mat, down_mat):
    gate_pre = jnp.dot(inputs, gate_mat, preferred_element_type=jnp.float32)
    up_pre = jnp.dot(inputs, up_mat, preferred_element_type=jnp.float32)
    gate_part = jnp.minimum(gate_pre, clamp_limit)
    linear_part = jnp.clip(up_pre, -clamp_limit, clamp_limit)
    activation = (
        gate_part * jax.nn.sigmoid(sigmoid_slope * gate_part) * (linear_part + 1.0)
    ).astype(jnp.bfloat16)
    return jnp.dot(activation, down_mat, preferred_element_type=jnp.float32).astype(jnp.bfloat16)


def assemble(received, rows_groups, column_groups):
    tile_rows = received.shape[2]
    tile_columns = received.shape[3]
    sources = received.reshape(rows_groups, column_groups, tile_rows, tile_columns)
    return sources.transpose(0, 2, 1, 3).reshape(
        1, rows_groups * tile_rows, column_groups * tile_columns
    )


def shards(tokens, routes, route_weight, norm_gain, gate_weight, up_weight, down_weight):
    gain_column = norm_gain[None, :, None]
    gate_tiles = (gate_weight * gain_column).astype(jnp.bfloat16)
    up_tiles = (up_weight * gain_column).astype(jnp.bfloat16)
    down_tiles = down_weight.astype(jnp.bfloat16)
    rows_groups = lax.axis_size("fs")
    column_groups = lax.axis_size("tp")
    arrived = (
        lax.all_to_all(gate_tiles[:, None], ("fs", "tp"), split_axis=0, concat_axis=1, tiled=True),
        lax.all_to_all(up_tiles[:, None], ("fs", "tp"), split_axis=0, concat_axis=1, tiled=True),
        lax.all_to_all(down_tiles[:, None], ("fs", "tp"), split_axis=0, concat_axis=1, tiled=True),
    )
    gate_new = assemble(arrived[0], rows_groups, column_groups)
    up_new = assemble(arrived[1], rows_groups, column_groups)
    down_new = assemble(arrived[2], rows_groups, column_groups)
    experts = rows_groups * column_groups
    tok_rows, model_width = tokens.shape
    per_token = routes.shape[1]
    capacity = max(2, 3 * tok_rows * per_token // (2 * experts))
    values = tokens.astype(jnp.float32)
    squares = jnp.mean(values * values, axis=1, keepdims=True)
    normed = (values * lax.rsqrt(squares + norm_epsilon)).astype(jnp.bfloat16)
    flat_routes = routes.reshape(-1)
    onehot = (flat_routes[:, None] == jnp.arange(experts, dtype=jnp.int32)[None, :]).astype(
        jnp.int32
    )
    earlier = jnp.cumsum(onehot, axis=0) - onehot
    rank = jnp.sum(earlier * onehot, axis=1)
    slot_index = flat_routes * capacity + rank
    slot_numbers = jnp.arange(experts * capacity, dtype=jnp.int32)
    select = jnp.any(
        slot_index.reshape(tok_rows, per_token)[None, :, :] == slot_numbers[:, None, None], axis=2
    )
    buffer = jnp.dot(
        select.astype(jnp.bfloat16), normed, preferred_element_type=jnp.float32
    ).astype(jnp.bfloat16)
    buffer = buffer.reshape(experts, 1, capacity, model_width)
    slot_rows = lax.all_to_all(buffer, ("fs", "tp"), split_axis=0, concat_axis=1, tiled=True)
    sources = slot_rows.shape[1]
    count = slot_rows.shape[2]
    expert_out = feed(slot_rows.reshape(-1, model_width), gate_new[0], up_new[0], down_new[0])
    expert_out = expert_out.reshape(1, sources, count, model_width)
    returned = lax.all_to_all(expert_out, ("fs", "tp"), split_axis=1, concat_axis=0, tiled=True)
    returned = returned.reshape(experts * capacity, model_width)
    picked = returned[slot_index].reshape(tok_rows, per_token, model_width)
    mixed = jnp.sum(picked.astype(jnp.float32) * route_weight[:, :, None], axis=1).astype(
        jnp.bfloat16
    )
    return (gate_new, up_new, down_new, mixed)


def exchange_kernel(
    sizes, tokens, routes_t, weight_t, gain, gate, up, down,
    gate_out, up_out, down_out, mixed,
    gate_in, up_in, down_in, gains, in_tiles, out_tiles, in_mats, out_mat,
    arrived, normed, slots_out, slots_in, active, far_routes, far_weight,
    mix_high, mix_low, rows_out, rows_in, part_out, part_in,
    load_sem, store_sem, token_send, token_recv, route_send, route_recv,
    first_send, first_recv, near_send, near_recv, slot_send, slot_recv,
    second_send, second_recv, back_send, back_recv, part_send, part_recv,
):
    n_fs, n_tp, capacity = sizes
    n = n_fs * n_tp
    fs, tp = lax.axis_index("fs"), lax.axis_index("tp")
    tok_rows, width = tokens.shape
    tile_rows, tile_cols = gate_in.shape[1:]
    chunks, down_rows, lanes = out_tiles.shape[1:]
    down_cols = chunks * lanes
    block = n_tp * lanes
    per_token = routes_t.shape[0]

    planes = 4
    plane_fs = n_fs // planes
    plane = n // planes
    layer, place = fs // plane_fs, lax.rem(fs, plane_fs)
    spot = place * n_tp + tp

    def flip(turn):
        low = lax.rem(layer + turn, 2)
        high = lax.rem(layer // 2 + turn // 2, 2)
        return 2 * high + low

    def device(turn, shift):
        to_place = lax.rem(place + shift // n_tp, plane_fs)
        to_tp = lax.rem(tp + lax.rem(shift, n_tp), n_tp)
        return flip(turn) * plane_fs + to_place, to_tp, to_place * n_tp + to_tp

    def peer(step):
        turn = lax.rem(step // (n // 2) + 1, 2) * 2 + lax.rem(step, 2)
        to_fs, to_tp, _ = device(turn, lax.rem(step // 2, plane))
        return to_fs, to_tp, to_fs * n_tp + to_tp

    def remote(source, target, send, recv, to):
        return pltpu.make_async_remote_copy(
            src_ref=source,
            dst_ref=target,
            send_sem=send,
            recv_sem=recv,
            device_id=(to[0], to[1]),
            device_id_type=MESH,
        )

    barrier = pltpu.get_barrier_semaphore()

    def greet(step, carry):
        to = peer(lax.rem(step + n // 2 + 1, n))
        pl.semaphore_signal(barrier, inc=1, device_id=(to[0], to[1]), device_id_type=MESH)
        return carry

    loads = [
        pltpu.make_async_copy(gate, gate_in, load_sem.at[0]),
        pltpu.make_async_copy(up, up_in, load_sem.at[1]),
        pltpu.make_async_copy(down, down_in, load_sem.at[2]),
    ]
    for load in loads:
        load.start()
    lax.fori_loop(0, n - 1, greet, 0)

    for i in range(tile_rows // lanes):
        gains[i * lanes : (i + 1) * lanes, :] = jnp.transpose(
            jnp.broadcast_to(gain[i : i + 1, :], (tile_cols, lanes))
        )

    def token_copy(turn, source):
        to = 1 if turn == 3 else turn
        return remote(
            source, arrived.at[turn - 1], token_send.at[turn - 1], token_recv.at[turn - 1], device(to, 0)
        )

    def route_copy(turn):
        return remote(
            routes_t, far_routes.at[turn - 1], route_send.at[turn - 1], route_recv.at[turn - 1], device(turn, 0)
        )

    weight_copy = remote(weight_t, far_weight, route_send.at[3], route_recv.at[3], device(2, 0))
    token_copies = [
        token_copy(1, tokens),
        token_copy(2, tokens),
        token_copy(3, arrived.at[1]),
    ]
    route_copies = [route_copy(1), route_copy(2), route_copy(3), weight_copy]

    def first_copy(to):
        return remote(
            in_tiles.at[to[2]],
            in_mats.at[
                :,
                pl.ds(pl.multiple_of(fs * tile_rows, tile_rows), tile_rows),
                pl.ds(pl.multiple_of(tp * tile_cols, tile_cols), tile_cols),
            ],
            first_send,
            first_recv,
            to,
        )

    own_rows = pl.ds(pl.multiple_of(fs * down_rows, down_rows), down_rows)
    own_lanes = pl.ds(pl.multiple_of(tp * lanes, lanes), lanes)

    def near_copy(to):
        return remote(
            out_tiles.at[to[2]], out_mat.at[:, own_rows, own_lanes], near_send, near_recv, to
        )

    def second_copy(c, to):
        return remote(
            out_tiles.at[to[2], c],
            out_mat.at[c, own_rows, own_lanes],
            second_send.at[c],
            second_recv.at[c],
            to,
        )

    def cast_first(step):
        e = peer(step)[2]
        in_tiles[e, 0] = (gate_in[e] * gains[...]).astype(jnp.bfloat16)
        in_tiles[e, 1] = (up_in[e] * gains[...]).astype(jnp.bfloat16)

    def cast_second(step):
        e = peer(step)[2]
        for c in range(chunks):
            out_tiles[e, c] = down_in[e, :, c * lanes : (c + 1) * lanes].astype(jnp.bfloat16)

    def send_first(step, carry):
        cast_first(step + 1)
        first_copy(peer(step)).start()
        return carry

    before = (
        lax.broadcasted_iota(jnp.int32, (tok_rows, tok_rows), 0)
        < lax.broadcasted_iota(jnp.int32, (tok_rows, tok_rows), 1)
    ).astype(jnp.float32).astype(jnp.bfloat16)

    def named_in(turn, paths, shares):
        experts = lax.broadcasted_iota(jnp.int32, (plane, tok_rows), 0) + flip(turn) * plane
        named = jnp.zeros((plane, tok_rows), jnp.float32)
        scaled = jnp.zeros((plane, tok_rows), jnp.float32)
        for k in range(per_token):
            hit = paths[k : k + 1, :] == experts
            named = named + hit.astype(jnp.float32)
            if shares is not None:
                scaled = scaled + jnp.where(hit, shares[k : k + 1, :], 0.0)
        rank = jnp.dot(named.astype(jnp.bfloat16), before, preferred_element_type=jnp.float32)
        rank = jnp.where(named > 0.5, rank, -1.0)
        number = lax.broadcasted_iota(jnp.int32, (plane, capacity, tok_rows), 1).astype(jnp.float32)
        return (rank[:, None, :] == number).astype(jnp.float32), scaled

    def normalize(turn, rows_ref):
        values = rows_ref[...].astype(jnp.float32)
        squares = jnp.mean(values * values, axis=1, keepdims=True)
        normed[turn] = (values * lax.rsqrt(squares + norm_epsilon)).astype(jnp.bfloat16)

    def fill_slots(turn, paths):
        select, _ = named_in(0, paths, None)
        rows = jnp.dot(
            select.reshape(plane * capacity, tok_rows).astype(jnp.bfloat16),
            normed[turn],
            preferred_element_type=jnp.float32,
        )
        slots_out[:, turn] = rows.reshape(plane, capacity, width).astype(jnp.bfloat16)

    def fill_mix(q, paths, shares):
        for turn in range(2):
            select, scaled = named_in(turn, paths, shares)
            picks = jnp.transpose(
                (select * scaled[:, None, :]).reshape(plane * capacity, tok_rows)
            )
            high = picks.astype(jnp.bfloat16)
            cols = slice(turn * plane * capacity, (turn + 1) * plane * capacity)
            mix_high[q, :, cols] = high
            mix_low[q, :, cols] = (picks - high.astype(jnp.float32)).astype(jnp.bfloat16)

    def slot_copy(to):
        return remote(slots_out.at[to[2]], slots_in.at[spot], slot_send, slot_recv, to)

    normalize(0, tokens)
    pl.semaphore_wait(barrier, n - 1)
    for each in route_copies:
        each.start()
    token_copies[1].start()
    token_copies[0].start()

    early = 3 * n // 16
    loads[0].wait()
    loads[1].wait()
    cast_first(0)
    lax.fori_loop(0, early, send_first, 0)

    for each in route_copies:
        each.wait_recv()
    fill_slots(0, routes_t)
    token_copies[1].wait_recv()
    token_copies[2].start()
    lax.fori_loop(early, n // 2, send_first, 0)
    normalize(2, arrived.at[1])
    fill_slots(2, far_routes.at[1])
    token_copies[0].wait_recv()
    normalize(1, arrived.at[0])
    fill_slots(1, far_routes.at[0])
    cast_first(n // 2 + 1)
    lax.fori_loop(n // 2 + 1, n // 2 + n // 4, send_first, 0)
    token_copies[2].wait_recv()
    normalize(3, arrived.at[2])
    fill_slots(3, far_routes.at[2])

    def send_slots(step, carry):
        slot_copy(device(0, step)).start()
        return carry

    slots_in[spot] = slots_out[spot]
    lax.fori_loop(1, plane, send_slots, 0)
    lax.fori_loop(n // 2 + n // 4, n - 1, send_first, 0)
    first_copy(peer(n - 1)).start()

    me = fs * n_tp + tp
    mine_rows = pl.ds(pl.multiple_of(fs * tile_rows, tile_rows), tile_rows)
    mine_cols = pl.ds(pl.multiple_of(tp * tile_cols, tile_cols), tile_cols)
    in_mats[0, mine_rows, mine_cols] = in_tiles[me, 0]
    in_mats[1, mine_rows, mine_cols] = in_tiles[me, 1]

    loads[2].wait()
    cast_second(0)

    def send_second(step, carry):
        cast_second(step + 1)
        second_copy(0, peer(step)).start()
        return carry

    lax.fori_loop(0, n // 2, send_second, 0)
    out_mat[:, own_rows, own_lanes] = out_tiles[me]
    cast_second(n // 2 + 1)

    def send_near(step, carry):
        cast_second(step + 1)
        near_copy(peer(step)).start()
        return carry

    lax.fori_loop(n // 2 + 1, n - 1, send_near, 0)
    near_copy(peer(n - 1)).start()

    def send_chunk(c):
        def send_one(step, carry):
            second_copy(c, peer(step)).start()
            return carry

        lax.fori_loop(0, n // 2, send_one, 0)

    send_chunk(1)
    fill_mix(0, routes_t, weight_t)
    fill_mix(1, far_routes.at[1], far_weight)

    near = device(1, 0)

    def take(size_ref, send, recv):
        return remote(size_ref, size_ref, send, recv, near)

    slots_all = take(slots_in.at[pl.ds(0, plane - 1)], slot_send, slot_recv)
    first_all = take(in_tiles.at[pl.ds(0, n - 1)], first_send, first_recv)
    near_all = take(out_tiles.at[pl.ds(0, n // 2 - 1)], near_send, near_recv)

    def second_all(c):
        return take(out_tiles.at[pl.ds(0, n // 2), c], second_send.at[c], second_recv.at[c])

    def back_all(c):
        return take(
            rows_in.at[c, :, pl.ds(0, n // 2 - 1)], back_send.at[c], back_recv.at[c]
        )

    slots_all.wait_recv()
    first_all.wait_recv()
    stores = [
        pltpu.make_async_copy(in_mats.at[0], gate_out.at[0], store_sem.at[0]),
        pltpu.make_async_copy(in_mats.at[1], up_out.at[0], store_sem.at[1]),
    ]
    stores[0].start()
    stores[1].start()

    group = active.shape[1]
    held = group // (planes * capacity)

    def activate(g, carry):
        inputs = slots_in[pl.ds(g * held, held)].astype(jnp.float32)
        inputs = inputs.reshape(group, width).astype(jnp.bfloat16)
        gate_pre = jnp.dot(inputs, in_mats[0], preferred_element_type=jnp.float32)
        up_pre = jnp.dot(inputs, in_mats[1], preferred_element_type=jnp.float32)
        gate_part = jnp.minimum(gate_pre, clamp_limit)
        linear_part = jnp.clip(up_pre, -clamp_limit, clamp_limit)
        active[g] = (
            gate_part * jax.nn.sigmoid(sigmoid_slope * gate_part) * (linear_part + 1.0)
        ).astype(jnp.bfloat16)
        return carry

    lax.fori_loop(0, active.shape[0], activate, 0)
    near_all.wait_recv()

    def back_copy(c, turn, shift):
        to = device(turn, shift)
        return remote(
            rows_out.at[c, turn, to[2]],
            rows_in.at[c, :, turn * plane + spot],
            back_send.at[c],
            back_recv.at[c],
            to,
        )

    def store_down(c, k):
        return pltpu.make_async_copy(
            out_mat.at[c, :, k * lanes : (k + 1) * lanes],
            down_out.at[0, :, k * down_cols + c * lanes : k * down_cols + (c + 1) * lanes],
            store_sem.at[2 + c * n_tp + k],
        )

    def project(c):
        second_all(c).wait_recv()

        def project_group(g, carry):
            rows = jnp.dot(active[g], out_mat[c], preferred_element_type=jnp.float32)
            rows = rows.reshape(held, planes, capacity, block).astype(jnp.bfloat16)
            spots = pl.ds(g * held, held)
            for turn in range(2):
                for q in range(2):
                    rows_out[c, turn, spots, q] = rows[:, 2 * q + turn]
            return carry

        lax.fori_loop(0, active.shape[0], project_group, 0)
        for k in range(n_tp):
            store_down(c, k).start()

        def send_back(step, carry):
            back_copy(c, 1, step).start()
            return carry

        def send_side(step, carry):
            back_copy(c, 0, step).start()
            return carry

        lax.fori_loop(1, plane, send_side, 0)
        lax.fori_loop(0, plane, send_back, 0)
        for q in range(2):
            rows_in[c, q, spot] = rows_out[c, 0, spot, q]

    span = 2 * plane * capacity

    def combine(c, q):
        rows = rows_in[c, q].astype(jnp.float32).reshape(span, block).astype(jnp.bfloat16)
        total = jnp.dot(mix_high[q], rows, preferred_element_type=jnp.float32)
        return total + jnp.dot(mix_low[q], rows, preferred_element_type=jnp.float32)

    def part_copy(c):
        return remote(part_out.at[c], part_in.at[c], part_send.at[c], part_recv.at[c], device(2, 0))

    def give(c):
        back_all(c).wait_recv()
        part_out[c] = combine(c, 1).astype(jnp.bfloat16)

    def finish(c):
        total = combine(c, 0)
        part_copy(c).wait_recv()
        total = (total + part_in[c].astype(jnp.float32)).astype(jnp.bfloat16)
        for k in range(n_tp):
            start = k * down_cols + c * lanes
            mixed[:, start : start + lanes] = total[:, k * lanes : (k + 1) * lanes]

    for c in range(chunks):
        project(c)
        if c + 2 < chunks:
            send_chunk(c + 2)
        if c > 0:
            give(c - 1)
            part_copy(c - 1).start()
    give(chunks - 1)
    part_copy(chunks - 1).start()
    for c in range(chunks):
        finish(c)

    first_all.wait_send()
    near_all.wait_send()
    slots_all.wait_send()
    for c in range(chunks):
        second_all(c).wait_send()
        back_all(c).wait_send()
        part_copy(c).wait_send()
    for each in token_copies + route_copies:
        each.wait_send()
    for store in stores:
        store.wait()
    for c in range(chunks):
        for k in range(n_tp):
            store_down(c, k).wait()


def direct_shards(
    tokens, routes, route_weight, norm_gain, gate_weight, up_weight, down_weight
):
    n_fs, n_tp = lax.axis_size("fs"), lax.axis_size("tp")
    n = n_fs * n_tp
    tok_rows, width = tokens.shape
    tile_rows, tile_cols = gate_weight.shape[1:]
    down_rows, down_cols = down_weight.shape[1:]
    hidden = n_tp * tile_cols
    lanes = 128
    chunks = down_cols // lanes
    block = n_tp * lanes
    plane = n // 4
    per_token = routes.shape[1]
    capacity = max(2, 3 * tok_rows * per_token // (2 * n))
    bf16, f32 = jnp.bfloat16, jnp.float32
    whole = pl.BlockSpec(memory_space=pltpu.VMEM)
    apart = pl.BlockSpec(memory_space=pl.ANY)
    dma = pltpu.SemaphoreType.DMA
    groups = 4
    return pl.pallas_call(
        functools.partial(exchange_kernel, (n_fs, n_tp, capacity)),
        out_shape=(
            jax.ShapeDtypeStruct((1, width, hidden), bf16),
            jax.ShapeDtypeStruct((1, width, hidden), bf16),
            jax.ShapeDtypeStruct((1, hidden, width), bf16),
            jax.ShapeDtypeStruct((tok_rows, width), bf16),
        ),
        in_specs=[whole] * 4 + [apart] * 3,
        out_specs=(apart, apart, apart, whole),
        scratch_shapes=[
            pltpu.VMEM((n, tile_rows, tile_cols), f32),
            pltpu.VMEM((n, tile_rows, tile_cols), f32),
            pltpu.VMEM((n, down_rows, down_cols), f32),
            pltpu.VMEM((tile_rows, tile_cols), f32),
            pltpu.VMEM((n, 2, tile_rows, tile_cols), bf16),
            pltpu.VMEM((n, chunks, down_rows, lanes), bf16),
            pltpu.VMEM((2, width, hidden), bf16),
            pltpu.VMEM((chunks, hidden, block), bf16),
            pltpu.VMEM((3, tok_rows, width), bf16),
            pltpu.VMEM((4, tok_rows, width), bf16),
            pltpu.VMEM((plane, 4, capacity, width), bf16),
            pltpu.VMEM((plane, 4, capacity, width), bf16),
            pltpu.VMEM((groups, n * capacity // groups, hidden), bf16),
            pltpu.VMEM((3, per_token, tok_rows), routes.dtype),
            pltpu.VMEM((per_token, tok_rows), f32),
            pltpu.VMEM((2, tok_rows, 2 * plane * capacity), bf16),
            pltpu.VMEM((2, tok_rows, 2 * plane * capacity), bf16),
            pltpu.VMEM((chunks, 2, plane, 2, capacity, block), bf16),
            pltpu.VMEM((chunks, 2, 2 * plane, capacity, block), bf16),
            pltpu.VMEM((chunks, tok_rows, block), bf16),
            pltpu.VMEM((chunks, tok_rows, block), bf16),
            dma((3,)),
            dma((2 + chunks * n_tp,)),
            dma((3,)),
            dma((3,)),
            dma((4,)),
            dma((4,)),
            dma,
            dma,
            dma,
            dma,
            dma,
            dma,
        ]
        + [dma((chunks,))] * 6,
        compiler_params=pltpu.CompilerParams(
            collective_id=0, has_side_effects=True, vmem_limit_bytes=60 * 1024 * 1024
        ),
    )(
        tokens,
        routes.T,
        route_weight.T,
        norm_gain.reshape(tile_rows // lanes, lanes),
        gate_weight,
        up_weight,
        down_weight,
    )


def aligned(mesh, tokens, routes, gate_weight, down_weight):
    n_fs, n_tp = mesh.shape["fs"], mesh.shape["tp"]
    n = n_fs * n_tp
    tok_rows = tokens.shape[0] // n
    capacity = max(2, 3 * tok_rows * routes.shape[1] // (2 * n))
    return (
        gate_weight.shape[0] == n
        and n_fs % 4 == 0
        and n % 32 == 0
        and capacity % 8 == 0
        and tok_rows % 128 == 0
        and tokens.shape[1] % 512 == 0
        and gate_weight.shape[1] // n_fs % 128 == 0
        and gate_weight.shape[2] // n_tp % 128 == 0
        and down_weight.shape[1] // n_fs % 16 == 0
        and down_weight.shape[2] // n_tp % 128 == 0
    )


def solution(mesh):
    placed = (
        P(("fs", "tp"), None),
        P(("fs", "tp"), None),
        P(("fs", "tp"), None),
        P("fs"),
        P(None, "fs", "tp"),
        P(None, "fs", "tp"),
        P(None, "fs", "tp"),
    )

    def run(tokens, routes, route_weight, norm_gain, gate_weight, up_weight, down_weight):
        direct = aligned(mesh, tokens, routes, gate_weight, down_weight)
        return jax.shard_map(
            direct_shards if direct else shards,
            mesh=mesh,
            in_specs=placed,
            out_specs=(
                P(("fs", "tp"), None, None),
                P(("fs", "tp"), None, None),
                P(("fs", "tp"), None, None),
                P(("fs", "tp"), None),
            ),
            check_vma=False,
        )(tokens, routes, route_weight, norm_gain, gate_weight, up_weight, down_weight)

    return run
```

profile of v0, /device:TPU:8, one launch (start us, length us, event | category | flops | bytes accessed | tf_op | source)
XLA Modules:
  0.0 234.4 jit_solution(11424864860246608917)
XLA Ops:
  0.6 226.0 %shard_map.102 = (bf16[1,2048,512]{2,1,0:T(8,128)(2,1)}, bf16[1,2048,512]{2,1,0:T(8,128)(2,1)}, bf16[1,512,2048]{2,1,0:T(8,128)(2,1)}, bf16[128,2048]{1,0:T(8,128)(2,1)}) custom-call(bf16[128,2048]{1,0:T(8,128)(2,1)} %tokens.1, s32[4,128]{1,0:T(4,128)} %bitcast.3, f32[4,128]{1,0:T(4,128)} %bitcast.4, f32[2,128]{1,0:T(2,128)} %bitcast.5, ...), custom_call_target="tpu_custom_call" | custom-call | tf_op jit(solution)/shard_map/pallas_call | solution.py:506
  226.7 0.0 copy-start.1
  226.7 3.2 %copy.15 = bf16[1,2048,512]{2,1,0:T(8,128)(2,1)} copy(bf16[1,2048,512]{2,1,0:T(8,128)(2,1)} %get-tuple-element.8) | data formatting | bytes 4194304
  229.9 0.0 copy-done.1
  229.9 0.0 copy-start
  229.9 1.3 copy.16
  231.2 1.0 copy-done
  232.2 0.0 copy-start.2
  232.2 1.3 copy.17
  233.6 0.1 copy-done.2
  233.6 0.8 copy.18
Async XLA Ops:
  226.7 3.2 %copy-start.1 = (bf16[1,2048,512]{2,1,0:T(8,128)(2,1)S(1)}, bf16[1,2048,512]{2,1,0:T(8,128)(2,1)}, u32[]{:S(2)}) copy-start(bf16[1,2048,512]{2,1,0:T(8,128)(2,1)} %get-tuple-element.9) | copy-start | bytes 6291460
  229.9 2.3 %copy-start = (bf16[1,512,2048]{2,1,0:T(8,128)(2,1)S(1)}, bf16[1,512,2048]{2,1,0:T(8,128)(2,1)}, u32[]{:S(2)}) copy-start(bf16[1,512,2048]{2,1,0:T(8,128)(2,1)} %get-tuple-element.10) | copy-start | bytes 6291460
  232.2 1.4 copy-start.2
where the time goes:
time: 235 us; the launch traced here: 234 us
  Pallas kernels  226 us (96%)
  local copies, waits for them, and re-layouts  7.73 us (3%)
    pallas_call x1, Pallas kernels, direct_shards(): pl.pallas_call(functools.partial(exchange_kernel, (n_fs, n_tp, capacity))...  226 us
    unnamed x10, local copies, waits for them, and re-layouts  7.73 us

commit v1 on v0

--- a/solution.py
+++ b/solution.py
@@ -85,12 +85,12 @@
 
 
 def exchange_kernel(
-    sizes, tokens, routes_t, weight_t, gain, gate, up, down,
-    gate_out, up_out, down_out, mixed,
-    gate_in, up_in, down_in, gains, in_tiles, out_tiles, in_mats, out_mat,
+    sizes, tokens_far, routes_far, weight_far, gain_far, gate, up, down,
+    in_mats, out_mat, mixed,
+    tokens, routes_t, weight_t, gain, gate_in, up_in, down_in, gains, in_tiles, out_tiles,
     arrived, normed, slots_out, slots_in, active, far_routes, far_weight,
     mix_high, mix_low, rows_out, rows_in, part_out, part_in,
-    load_sem, store_sem, token_send, token_recv, route_send, route_recv,
+    load_sem, token_send, token_recv, route_send, route_recv,
     first_send, first_recv, near_send, near_recv, slot_send, slot_recv,
     second_send, second_recv, back_send, back_recv, part_send, part_recv,
 ):
@@ -121,8 +121,9 @@
         return flip(turn) * plane_fs + to_place, to_tp, to_place * n_tp + to_tp
 
     def peer(step):
-        turn = lax.rem(step // (n // 2) + 1, 2) * 2 + lax.rem(step, 2)
-        to_fs, to_tp, _ = device(turn, lax.rem(step // 2, plane))
+        crossing = 1 - lax.rem(step, 2)
+        at = lax.rem(step // 2 + 1 - crossing, n // 2)
+        to_fs, to_tp, _ = device(2 * crossing + lax.rem(at, 2), at // 2)
         return to_fs, to_tp, to_fs * n_tp + to_tp
 
     def remote(source, target, send, recv, to):
@@ -138,19 +139,30 @@
     barrier = pltpu.get_barrier_semaphore()
 
     def greet(step, carry):
-        to = peer(lax.rem(step + n // 2 + 1, n))
+        to = peer(step)
         pl.semaphore_signal(barrier, inc=1, device_id=(to[0], to[1]), device_id_type=MESH)
         return carry
 
     loads = [
-        pltpu.make_async_copy(gate, gate_in, load_sem.at[0]),
-        pltpu.make_async_copy(up, up_in, load_sem.at[1]),
-        pltpu.make_async_copy(down, down_in, load_sem.at[2]),
+        pltpu.make_async_copy(source, target, load_sem.at[i])
+        for i, (source, target) in enumerate(
+            [
+                (gain_far, gain),
+                (routes_far, routes_t),
+                (weight_far, weight_t),
+                (tokens_far, tokens),
+                (gate, gate_in),
+                (up, up_in),
+                (down, down_in),
+            ]
+        )
     ]
     for load in loads:
         load.start()
     lax.fori_loop(0, n - 1, greet, 0)
 
+    for load in loads[:4]:
+        load.wait()
     for i in range(tile_rows // lanes):
         gains[i * lanes : (i + 1) * lanes, :] = jnp.transpose(
             jnp.broadcast_to(gain[i : i + 1, :], (tile_cols, lanes))
@@ -264,8 +276,21 @@
             mix_high[q, :, cols] = high
             mix_low[q, :, cols] = (picks - high.astype(jnp.float32)).astype(jnp.bfloat16)
 
-    def slot_copy(to):
-        return remote(slots_out.at[to[2]], slots_in.at[spot], slot_send, slot_recv, to)
+    def slot_copy(turn, to):
+        return remote(
+            slots_out.at[to[2], turn], slots_in.at[spot, turn], slot_send, slot_recv, to
+        )
+
+    def send_slots(turn):
+        def send_one(step, carry):
+            slot_copy(turn, device(0, step)).start()
+            return carry
+
+        lax.fori_loop(1, plane, send_one, 0)
+        slots_in[spot, turn] = slots_out[spot, turn]
+
+    def send_some(start, stop):
+        lax.fori_loop(start, stop, send_first, 0)
 
     normalize(0, tokens)
     pl.semaphore_wait(barrier, n - 1)
@@ -273,38 +298,32 @@
         each.start()
     token_copies[1].start()
     token_copies[0].start()
-
-    early = 3 * n // 16
-    loads[0].wait()
-    loads[1].wait()
+    fill_slots(0, routes_t)
+    loads[4].wait()
+    loads[5].wait()
     cast_first(0)
-    lax.fori_loop(0, early, send_first, 0)
-
+    send_some(0, n // 8)
+    send_slots(0)
+    send_some(n // 8, 3 * n // 8)
     for each in route_copies:
         each.wait_recv()
-    fill_slots(0, routes_t)
     token_copies[1].wait_recv()
     token_copies[2].start()
-    lax.fori_loop(early, n // 2, send_first, 0)
     normalize(2, arrived.at[1])
     fill_slots(2, far_routes.at[1])
+    send_some(3 * n // 8, n // 2)
+    send_slots(2)
     token_copies[0].wait_recv()
     normalize(1, arrived.at[0])
     fill_slots(1, far_routes.at[0])
-    cast_first(n // 2 + 1)
-    lax.fori_loop(n // 2 + 1, n // 2 + n // 4, send_first, 0)
+    send_some(n // 2, 5 * n // 8)
+    send_slots(1)
     token_copies[2].wait_recv()
     normalize(3, arrived.at[2])
     fill_slots(3, far_routes.at[2])
-
-    def send_slots(step, carry):
-        slot_copy(device(0, step)).start()
-        return carry
-
-    slots_in[spot] = slots_out[spot]
-    lax.fori_loop(1, plane, send_slots, 0)
-    lax.fori_loop(n // 2 + n // 4, n - 1, send_first, 0)
-    first_copy(peer(n - 1)).start()
+    send_some(5 * n // 8, 6 * n // 8)
+    send_slots(3)
+    send_some(6 * n // 8, n - 1)
 
     me = fs * n_tp + tp
     mine_rows = pl.ds(pl.multiple_of(fs * tile_rows, tile_rows), tile_rows)
@@ -312,29 +331,24 @@
     in_mats[0, mine_rows, mine_cols] = in_tiles[me, 0]
     in_mats[1, mine_rows, mine_cols] = in_tiles[me, 1]
 
-    loads[2].wait()
+    loads[6].wait()
     cast_second(0)
+    cast_second(1)
 
     def send_second(step, carry):
-        cast_second(step + 1)
-        second_copy(0, peer(step)).start()
+        cast_second(2 * step + 2)
+        second_copy(0, peer(2 * step)).start()
+        cast_second(2 * step + 3)
+        near_copy(peer(2 * step + 1)).start()
         return carry
 
-    lax.fori_loop(0, n // 2, send_second, 0)
+    lax.fori_loop(0, n // 2 - 1, send_second, 0)
+    second_copy(0, peer(n - 2)).start()
     out_mat[:, own_rows, own_lanes] = out_tiles[me]
-    cast_second(n // 2 + 1)
-
-    def send_near(step, carry):
-        cast_second(step + 1)
-        near_copy(peer(step)).start()
-        return carry
-
-    lax.fori_loop(n // 2 + 1, n - 1, send_near, 0)
-    near_copy(peer(n - 1)).start()
 
     def send_chunk(c):
         def send_one(step, carry):
-            second_copy(c, peer(step)).start()
+            second_copy(c, peer(2 * step)).start()
             return carry
 
         lax.fori_loop(0, n // 2, send_one, 0)
@@ -362,12 +376,6 @@
 
     slots_all.wait_recv()
     first_all.wait_recv()
-    stores = [
-        pltpu.make_async_copy(in_mats.at[0], gate_out.at[0], store_sem.at[0]),
-        pltpu.make_async_copy(in_mats.at[1], up_out.at[0], store_sem.at[1]),
-    ]
-    stores[0].start()
-    stores[1].start()
 
     group = active.shape[1]
     held = group // (planes * capacity)
@@ -397,13 +405,6 @@
             to,
         )
 
-    def store_down(c, k):
-        return pltpu.make_async_copy(
-            out_mat.at[c, :, k * lanes : (k + 1) * lanes],
-            down_out.at[0, :, k * down_cols + c * lanes : k * down_cols + (c + 1) * lanes],
-            store_sem.at[2 + c * n_tp + k],
-        )
-
     def project(c):
         second_all(c).wait_recv()
 
@@ -417,8 +418,6 @@
             return carry
 
         lax.fori_loop(0, active.shape[0], project_group, 0)
-        for k in range(n_tp):
-            store_down(c, k).start()
 
         def send_back(step, carry):
             back_copy(c, 1, step).start()
@@ -476,11 +475,35 @@
         part_copy(c).wait_send()
     for each in token_copies + route_copies:
         each.wait_send()
-    for store in stores:
-        store.wait()
+
+
+def keep_kernel(in_mats, out_mat, rows, gate_out, up_out, down_out, mixed, sem):
+    chunks, _, block = out_mat.shape
+    n_tp = block // 128
+    lanes = block // n_tp
+    down_cols = chunks * lanes
+    copies = [
+        (in_mats.at[0], gate_out.at[0]),
+        (in_mats.at[1], up_out.at[0]),
+        (rows, mixed),
+    ]
     for c in range(chunks):
         for k in range(n_tp):
-            store_down(c, k).wait()
+            start = k * down_cols + c * lanes
+            copies.append(
+                (
+                    out_mat.at[c, :, k * lanes : (k + 1) * lanes],
+                    down_out.at[0, :, start : start + lanes],
+                )
+            )
+    copies = [
+        pltpu.make_async_copy(source, target, sem.at[i])
+        for i, (source, target) in enumerate(copies)
+    ]
+    for copy in copies:
+        copy.start()
+    for copy in copies:
+        copy.wait()
 
 
 def direct_shards(
@@ -500,28 +523,29 @@
     capacity = max(2, 3 * tok_rows * per_token // (2 * n))
     bf16, f32 = jnp.bfloat16, jnp.float32
     whole = pl.BlockSpec(memory_space=pltpu.VMEM)
-    apart = pl.BlockSpec(memory_space=pl.ANY)
+    apart = pl.BlockSpec(memory_space=pltpu.HBM)
     dma = pltpu.SemaphoreType.DMA
     groups = 4
-    return pl.pallas_call(
+    in_mats, out_mat, rows = pl.pallas_call(
         functools.partial(exchange_kernel, (n_fs, n_tp, capacity)),
         out_shape=(
-            jax.ShapeDtypeStruct((1, width, hidden), bf16),
-            jax.ShapeDtypeStruct((1, width, hidden), bf16),
-            jax.ShapeDtypeStruct((1, hidden, width), bf16),
-            jax.ShapeDtypeStruct((tok_rows, width), bf16),
+            pltpu.VMEM((2, width, hidden), bf16),
+            pltpu.VMEM((chunks, hidden, block), bf16),
+            pltpu.VMEM((tok_rows, width), bf16),
         ),
-        in_specs=[whole] * 4 + [apart] * 3,
-        out_specs=(apart, apart, apart, whole),
+        in_specs=[apart] * 7,
+        out_specs=(whole, whole, whole),
         scratch_shapes=[
+            pltpu.VMEM((tok_rows, width), tokens.dtype),
+            pltpu.VMEM((per_token, tok_rows), routes.dtype),
+            pltpu.VMEM((per_token, tok_rows), f32),
+            pltpu.VMEM((tile_rows // lanes, lanes), f32),
             pltpu.VMEM((n, tile_rows, tile_cols), f32),
             pltpu.VMEM((n, tile_rows, tile_cols), f32),
             pltpu.VMEM((n, down_rows, down_cols), f32),
             pltpu.VMEM((tile_rows, tile_cols), f32),
             pltpu.VMEM((n, 2, tile_rows, tile_cols), bf16),
             pltpu.VMEM((n, chunks, down_rows, lanes), bf16),
-            pltpu.VMEM((2, width, hidden), bf16),
-            pltpu.VMEM((chunks, hidden, block), bf16),
             pltpu.VMEM((3, tok_rows, width), bf16),
             pltpu.VMEM((4, tok_rows, width), bf16),
             pltpu.VMEM((plane, 4, capacity, width), bf16),
@@ -535,8 +559,7 @@
             pltpu.VMEM((chunks, 2, 2 * plane, capacity, block), bf16),
             pltpu.VMEM((chunks, tok_rows, block), bf16),
             pltpu.VMEM((chunks, tok_rows, block), bf16),
-            dma((3,)),
-            dma((2 + chunks * n_tp,)),
+            dma((7,)),
             dma((3,)),
             dma((3,)),
             dma((4,)),
@@ -550,7 +573,7 @@
         ]
         + [dma((chunks,))] * 6,
         compiler_params=pltpu.CompilerParams(
-            collective_id=0, has_side_effects=True, vmem_limit_bytes=60 * 1024 * 1024
+            collective_id=0, has_side_effects=True, vmem_limit_bytes=50 * 1024 * 1024
         ),
     )(
         tokens,
@@ -561,6 +584,19 @@
         up_weight,
         down_weight,
     )
+    return pl.pallas_call(
+        keep_kernel,
+        out_shape=(
+            jax.ShapeDtypeStruct((1, width, hidden), bf16),
+            jax.ShapeDtypeStruct((1, width, hidden), bf16),
+            jax.ShapeDtypeStruct((1, hidden, width), bf16),
+            jax.ShapeDtypeStruct((tok_rows, width), bf16),
+        ),
+        in_specs=[whole] * 3,
+        out_specs=(apart,) * 4,
+        scratch_shapes=[dma((3 + chunks * n_tp,))],
+        compiler_params=pltpu.CompilerParams(vmem_limit_bytes=8 * 1024 * 1024),
+    )(in_mats, out_mat, rows)
 
 
 def aligned(mesh, tokens, routes, gate_weight, down_weight):

time: 235 us -> 210 us (0.89)
  Pallas kernels: 226 us -> 209 us
  local copies, waits for them, and re-layouts: 7.73 us -> 0 us
    pallas_call x1, Pallas kernels: 226 us -> 206 us  [direct_shards(): pl.pallas_call(functools.partial(exchange_kernel, (n_fs, n_tp, capacity))...]
    unnamed x10 -> x0, local copies, waits for them, and re-layouts: 7.73 us -> none
    pallas_call x0 -> x1, Pallas kernels: none -> 2.95 us  [direct_shards(): pl.pallas_call(keep_kernel, out_shape=(jax.ShapeDtypeStruct((1, width, hi...]
where the time goes in v1:
time: 210 us
  Pallas kernels  209 us (100%)
    pallas_call x1, Pallas kernels, direct_shards(): pl.pallas_call(functools.partial(exchange_kernel, (n_fs, n_tp, capacity))...  206 us

profile of v1, /device:TPU:8, one launch (start us, length us, event | category | flops | bytes accessed | tf_op | source)
XLA Modules:
  0.0 209.7 jit_solution(16510670209885011343)
XLA Ops:
  0.6 206.1 %shard_map.102 = (bf16[2,2048,512]{2,1,0:T(8,128)(2,1)S(1)}, bf16[4,512,512]{2,1,0:T(8,128)(2,1)S(1)}, bf16[128,2048]{1,0:T(8,128)(2,1)S(1)}) custom-call(bf16[128,2048]{1,0:T(8,128)(2,1)} %tokens_far.1, s32[4,128]{1,0:T(4,128)} %bitcast.3, f32[4,128]{1,0:T(4,128)} %bitcast.4, f32[2,128]{1,0:T(2,128)} %bitcast.5, f32[32,256,128]{2,1,0:T(8,128)} %gate.1, ...), custom_call_target="tpu_custom_call" | custom-call | tf_op jit(solution)/shard_map/pallas_call | solution.py:529
  206.7 2.9 %shard_map.103 = (bf16[1,2048,512]{2,1,0:T(8,128)(2,1)}, bf16[1,2048,512]{2,1,0:T(8,128)(2,1)}, bf16[1,512,2048]{2,1,0:T(8,128)(2,1)}, bf16[128,2048]{1,0:T(8,128)(2,1)}) custom-call(bf16[2,2048,512]{2,1,0:T(8,128)(2,1)S(1)} %get-tuple-element.7.in_mats, bf16[4,512,512]{2,1,0:T(8,128)(2,1)S(1)} %get-tuple-element.8.out_mat, ...), custom_call_target="tpu_custom_call" | custom-call | tf_op jit(solution)/shard_map/pallas_call | solution.py:587

commit v2 on v1

--- a/solution.py
+++ b/solution.py
@@ -89,10 +89,10 @@
     in_mats, out_mat, mixed,
     tokens, routes_t, weight_t, gain, gate_in, up_in, down_in, gains, in_tiles, out_tiles,
     arrived, normed, slots_out, slots_in, active, far_routes, far_weight,
-    mix_high, mix_low, rows_out, rows_in, part_out, part_in,
+    mix_high, mix_low, rows_out, rows_in, side_out, side_in, totals, part_out, part_in,
     load_sem, token_send, token_recv, route_send, route_recv,
     first_send, first_recv, near_send, near_recv, slot_send, slot_recv,
-    second_send, second_recv, back_send, back_recv, part_send, part_recv,
+    second_send, second_recv, back_send, back_recv, side_send, side_recv, part_send, part_recv,
 ):
     n_fs, n_tp, capacity = sizes
     n = n_fs * n_tp
@@ -121,9 +121,20 @@
         return flip(turn) * plane_fs + to_place, to_tp, to_place * n_tp + to_tp
 
     def peer(step):
+        paired = 1 - step // (n - 2)
+        step = step + (1 - 2 * lax.rem(step, 2)) * paired * 0
         crossing = 1 - lax.rem(step, 2)
         at = lax.rem(step // 2 + 1 - crossing, n // 2)
         to_fs, to_tp, _ = device(2 * crossing + lax.rem(at, 2), at // 2)
+        return to_fs, to_tp, to_fs * n_tp + to_tp
+
+    def cross(at):
+        to_fs, to_tp, _ = device(2 + lax.rem(at, 2), at // 2)
+        return to_fs, to_tp, to_fs * n_tp + to_tp
+
+    def close(at):
+        at = lax.rem(at + 1, n // 2)
+        to_fs, to_tp, _ = device(lax.rem(at, 2), at // 2)
         return to_fs, to_tp, to_fs * n_tp + to_tp
 
     def remote(source, target, send, recv, to):
@@ -179,13 +190,17 @@
             routes_t, far_routes.at[turn - 1], route_send.at[turn - 1], route_recv.at[turn - 1], device(turn, 0)
         )
 
-    weight_copy = remote(weight_t, far_weight, route_send.at[3], route_recv.at[3], device(2, 0))
+    def weight_copy(turn):
+        return remote(
+            weight_t, far_weight.at[turn - 1], route_send.at[turn + 2], route_recv.at[turn + 2], device(turn, 0)
+        )
+
     token_copies = [
         token_copy(1, tokens),
         token_copy(2, tokens),
         token_copy(3, arrived.at[1]),
     ]
-    route_copies = [route_copy(1), route_copy(2), route_copy(3), weight_copy]
+    route_copies = [copy(turn) for copy in (route_copy, weight_copy) for turn in (1, 2, 3)]
 
     def first_copy(to):
         return remote(
@@ -237,8 +252,10 @@
         < lax.broadcasted_iota(jnp.int32, (tok_rows, tok_rows), 1)
     ).astype(jnp.float32).astype(jnp.bfloat16)
 
-    def named_in(turn, paths, shares):
-        experts = lax.broadcasted_iota(jnp.int32, (plane, tok_rows), 0) + flip(turn) * plane
+    experts = lax.broadcasted_iota(jnp.int32, (plane, tok_rows), 0) + layer * plane
+    number = lax.broadcasted_iota(jnp.int32, (plane, capacity, tok_rows), 1).astype(jnp.float32)
+
+    def named_in(paths, shares):
         named = jnp.zeros((plane, tok_rows), jnp.float32)
         scaled = jnp.zeros((plane, tok_rows), jnp.float32)
         for k in range(per_token):
@@ -248,7 +265,6 @@
                 scaled = scaled + jnp.where(hit, shares[k : k + 1, :], 0.0)
         rank = jnp.dot(named.astype(jnp.bfloat16), before, preferred_element_type=jnp.float32)
         rank = jnp.where(named > 0.5, rank, -1.0)
-        number = lax.broadcasted_iota(jnp.int32, (plane, capacity, tok_rows), 1).astype(jnp.float32)
         return (rank[:, None, :] == number).astype(jnp.float32), scaled
 
     def normalize(turn, rows_ref):
@@ -257,7 +273,7 @@
         normed[turn] = (values * lax.rsqrt(squares + norm_epsilon)).astype(jnp.bfloat16)
 
     def fill_slots(turn, paths):
-        select, _ = named_in(0, paths, None)
+        select, _ = named_in(paths, None)
         rows = jnp.dot(
             select.reshape(plane * capacity, tok_rows).astype(jnp.bfloat16),
             normed[turn],
@@ -265,16 +281,12 @@
         )
         slots_out[:, turn] = rows.reshape(plane, capacity, width).astype(jnp.bfloat16)
 
-    def fill_mix(q, paths, shares):
-        for turn in range(2):
-            select, scaled = named_in(turn, paths, shares)
-            picks = jnp.transpose(
-                (select * scaled[:, None, :]).reshape(plane * capacity, tok_rows)
-            )
-            high = picks.astype(jnp.bfloat16)
-            cols = slice(turn * plane * capacity, (turn + 1) * plane * capacity)
-            mix_high[q, :, cols] = high
-            mix_low[q, :, cols] = (picks - high.astype(jnp.float32)).astype(jnp.bfloat16)
+    def fill_mix(turn, paths, shares):
+        select, scaled = named_in(paths, shares)
+        picks = jnp.transpose((select * scaled[:, None, :]).reshape(plane * capacity, tok_rows))
+        high = picks.astype(jnp.bfloat16)
+        mix_high[turn] = high
+        mix_low[turn] = (picks - high.astype(jnp.float32)).astype(jnp.bfloat16)
 
     def slot_copy(turn, to):
         return remote(
@@ -337,25 +349,31 @@
 
     def send_second(step, carry):
         cast_second(2 * step + 2)
-        second_copy(0, peer(2 * step)).start()
         cast_second(2 * step + 3)
-        near_copy(peer(2 * step + 1)).start()
+        second_copy(0, cross(step)).start()
         return carry
 
     lax.fori_loop(0, n // 2 - 1, send_second, 0)
-    second_copy(0, peer(n - 2)).start()
+    second_copy(0, cross(n // 2 - 1)).start()
+
+    def send_near(step, carry):
+        near_copy(close(step)).start()
+        return carry
+
+    lax.fori_loop(0, n // 2 - 1, send_near, 0)
     out_mat[:, own_rows, own_lanes] = out_tiles[me]
 
     def send_chunk(c):
         def send_one(step, carry):
-            second_copy(c, peer(2 * step)).start()
+            second_copy(c, cross(step)).start()
             return carry
 
         lax.fori_loop(0, n // 2, send_one, 0)
 
     send_chunk(1)
     fill_mix(0, routes_t, weight_t)
-    fill_mix(1, far_routes.at[1], far_weight)
+    for turn in range(1, planes):
+        fill_mix(turn, far_routes.at[turn - 1], far_weight.at[turn - 1])
 
     near = device(1, 0)
 
@@ -369,10 +387,8 @@
     def second_all(c):
         return take(out_tiles.at[pl.ds(0, n // 2), c], second_send.at[c], second_recv.at[c])
 
-    def back_all(c):
-        return take(
-            rows_in.at[c, :, pl.ds(0, n // 2 - 1)], back_send.at[c], back_recv.at[c]
-        )
+    def back_all(j):
+        return take(rows_in.at[j, pl.ds(0, plane - 1)], back_send.at[j], back_recv.at[j])
 
     slots_all.wait_recv()
     first_all.wait_recv()
@@ -395,84 +411,105 @@
     lax.fori_loop(0, active.shape[0], activate, 0)
     near_all.wait_recv()
 
-    def back_copy(c, turn, shift):
-        to = device(turn, shift)
-        return remote(
-            rows_out.at[c, turn, to[2]],
-            rows_in.at[c, :, turn * plane + spot],
-            back_send.at[c],
-            back_recv.at[c],
-            to,
-        )
+    pieces, piece = rows_out.shape[0], rows_out.shape[-1]
+    split = pieces // chunks
+
+    def back_copy(j, shift):
+        to = device(0, shift)
+        return remote(
+            rows_out.at[j, to[2]], rows_in.at[j, spot], back_send.at[j], back_recv.at[j], to
+        )
+
+    def side_copy(j):
+        return remote(side_out.at[j], side_in.at[j], side_send.at[j], side_recv.at[j], device(1, 0))
+
+    def part_copy(j):
+        return remote(part_out.at[j], part_in.at[j], part_send.at[j], part_recv.at[j], device(2, 0))
 
     def project(c):
         second_all(c).wait_recv()
-
-        def project_group(g, carry):
-            rows = jnp.dot(active[g], out_mat[c], preferred_element_type=jnp.float32)
-            rows = rows.reshape(held, planes, capacity, block).astype(jnp.bfloat16)
-            spots = pl.ds(g * held, held)
-            for turn in range(2):
-                for q in range(2):
-                    rows_out[c, turn, spots, q] = rows[:, 2 * q + turn]
-            return carry
-
-        lax.fori_loop(0, active.shape[0], project_group, 0)
-
-        def send_back(step, carry):
-            back_copy(c, 1, step).start()
-            return carry
-
-        def send_side(step, carry):
-            back_copy(c, 0, step).start()
-            return carry
-
-        lax.fori_loop(1, plane, send_side, 0)
-        lax.fori_loop(0, plane, send_back, 0)
+        for i in range(split):
+            j = c * split + i
+
+            def project_group(g, carry):
+                rows = jnp.dot(
+                    active[g],
+                    out_mat[c, :, i * piece : (i + 1) * piece],
+                    preferred_element_type=jnp.float32,
+                )
+                rows_out[j, pl.ds(g * held, held)] = rows.reshape(
+                    held, planes, capacity, piece
+                ).astype(jnp.bfloat16)
+                return carry
+
+            lax.fori_loop(0, active.shape[0], project_group, 0)
+
+            def send_back(step, carry):
+                back_copy(j, step).start()
+                return carry
+
+            lax.fori_loop(1, plane, send_back, 0)
+            rows_in[j, spot] = rows_out[j, spot]
+
+    span = plane * capacity
+
+    def combine(j, turn):
+        rows = rows_in[j, :, turn].astype(jnp.float32).reshape(span, piece).astype(jnp.bfloat16)
+        total = jnp.dot(mix_high[turn], rows, preferred_element_type=jnp.float32)
+        return total + jnp.dot(mix_low[turn], rows, preferred_element_type=jnp.float32)
+
+    def give_side(j):
+        back_all(j).wait_recv()
         for q in range(2):
-            rows_in[c, q, spot] = rows_out[c, 0, spot, q]
-
-    span = 2 * plane * capacity
-
-    def combine(c, q):
-        rows = rows_in[c, q].astype(jnp.float32).reshape(span, block).astype(jnp.bfloat16)
-        total = jnp.dot(mix_high[q], rows, preferred_element_type=jnp.float32)
-        return total + jnp.dot(mix_low[q], rows, preferred_element_type=jnp.float32)
-
-    def part_copy(c):
-        return remote(part_out.at[c], part_in.at[c], part_send.at[c], part_recv.at[c], device(2, 0))
-
-    def give(c):
-        back_all(c).wait_recv()
-        part_out[c] = combine(c, 1).astype(jnp.bfloat16)
-
-    def finish(c):
-        total = combine(c, 0)
-        part_copy(c).wait_recv()
-        total = (total + part_in[c].astype(jnp.float32)).astype(jnp.bfloat16)
-        for k in range(n_tp):
-            start = k * down_cols + c * lanes
+            side_out[j, q] = combine(j, 2 * q + 1).astype(jnp.bfloat16)
+        for q in range(1, -1, -1):
+            totals[j, q] = combine(j, 2 * q)
+            if q == 1:
+                side_copy(j).start()
+
+    def give_part(j):
+        side_copy(j).wait_recv()
+        part_out[j] = (totals[j, 1] + side_in[j, 1].astype(jnp.float32)).astype(jnp.bfloat16)
+        totals[j, 0] = totals[j, 0] + side_in[j, 0].astype(jnp.float32)
+        part_copy(j).start()
+
+    def finish(j):
+        part_copy(j).wait_recv()
+        total = (totals[j, 0] + part_in[j].astype(jnp.float32)).astype(jnp.bfloat16)
+        for k in range(piece // lanes):
+            slab = j % split * (piece // lanes) + k
+            start = slab * down_cols + j // split * lanes
             mixed[:, start : start + lanes] = total[:, k * lanes : (k + 1) * lanes]
+
+    def run(stage, c):
+        for i in range(split):
+            stage(c * split + i)
 
     for c in range(chunks):
         project(c)
+        if c > 0:
+            run(give_side, c - 1)
         if c + 2 < chunks:
             send_chunk(c + 2)
-        if c > 0:
-            give(c - 1)
-            part_copy(c - 1).start()
-    give(chunks - 1)
-    part_copy(chunks - 1).start()
-    for c in range(chunks):
-        finish(c)
+        if c > 1:
+            run(give_part, c - 2)
+    for i in range(split):
+        give_side((chunks - 1) * split + i)
+        if i == 0:
+            run(give_part, chunks - 2)
+    run(give_part, chunks - 1)
+    for j in range(pieces):
+        finish(j)
 
     first_all.wait_send()
     near_all.wait_send()
     slots_all.wait_send()
     for c in range(chunks):
         second_all(c).wait_send()
-        back_all(c).wait_send()
-        part_copy(c).wait_send()
+    for j in range(pieces):
+        back_all(j).wait_send()
+        side_copy(j).wait_send()
+        part_copy(j).wait_send()
     for each in token_copies + route_copies:
         each.wait_send()
 
@@ -519,6 +556,7 @@
     chunks = down_cols // lanes
     block = n_tp * lanes
     plane = n // 4
+    pieces, piece = chunks * 2, block // 2
     per_token = routes.shape[1]
     capacity = max(2, 3 * tok_rows * per_token // (2 * n))
     bf16, f32 = jnp.bfloat16, jnp.float32
@@ -552,18 +590,21 @@
             pltpu.VMEM((plane, 4, capacity, width), bf16),
             pltpu.VMEM((groups, n * capacity // groups, hidden), bf16),
             pltpu.VMEM((3, per_token, tok_rows), routes.dtype),
-            pltpu.VMEM((per_token, tok_rows), f32),
-            pltpu.VMEM((2, tok_rows, 2 * plane * capacity), bf16),
-            pltpu.VMEM((2, tok_rows, 2 * plane * capacity), bf16),
-            pltpu.VMEM((chunks, 2, plane, 2, capacity, block), bf16),
-            pltpu.VMEM((chunks, 2, 2 * plane, capacity, block), bf16),
-            pltpu.VMEM((chunks, tok_rows, block), bf16),
-            pltpu.VMEM((chunks, tok_rows, block), bf16),
+            pltpu.VMEM((3, per_token, tok_rows), f32),
+            pltpu.VMEM((4, tok_rows, plane * capacity), bf16),
+            pltpu.VMEM((4, tok_rows, plane * capacity), bf16),
+            pltpu.VMEM((pieces, plane, 4, capacity, piece), bf16),
+            pltpu.VMEM((pieces, plane, 4, capacity, piece), bf16),
+            pltpu.VMEM((pieces, 2, tok_rows, piece), bf16),
+            pltpu.VMEM((pieces, 2, tok_rows, piece), bf16),
+            pltpu.VMEM((pieces, 2, tok_rows, piece), f32),
+            pltpu.VMEM((pieces, tok_rows, piece), bf16),
+            pltpu.VMEM((pieces, tok_rows, piece), bf16),
             dma((7,)),
             dma((3,)),
             dma((3,)),
-            dma((4,)),
-            dma((4,)),
+            dma((6,)),
+            dma((6,)),
             dma,
             dma,
             dma,
@@ -571,9 +612,10 @@
             dma,
             dma,
         ]
-        + [dma((chunks,))] * 6,
+        + [dma((chunks,))] * 2
+        + [dma((pieces,))] * 6,
         compiler_params=pltpu.CompilerParams(
-            collective_id=0, has_side_effects=True, vmem_limit_bytes=50 * 1024 * 1024
+            collective_id=0, has_side_effects=True, vmem_limit_bytes=52 * 1024 * 1024
         ),
     )(
         tokens,

time: 210 us -> 203 us (0.967)
  Pallas kernels: 209 us -> 203 us
    pallas_call x1, Pallas kernels: 206 us -> 200 us  [direct_shards(): pl.pallas_call(functools.partial(exchange_kernel, (n_fs, n_tp, capacity))...]
where the time goes in v2:
time: 203 us
  Pallas kernels  203 us (100%)
    pallas_call x1, Pallas kernels, direct_shards(): pl.pallas_call(functools.partial(exchange_kernel, (n_fs, n_tp, capacity))...  200 us

profile of v2, /device:TPU:8, one launch (start us, length us, event | category | flops | bytes accessed | tf_op | source)
XLA Modules:
  0.0 203.2 jit_solution(13452399111315616997)
XLA Ops:
  0.6 199.6 %shard_map.102 = (bf16[2,2048,512]{2,1,0:T(8,128)(2,1)S(1)}, bf16[4,512,512]{2,1,0:T(8,128)(2,1)S(1)}, bf16[128,2048]{1,0:T(8,128)(2,1)S(1)}) custom-call(bf16[128,2048]{1,0:T(8,128)(2,1)} %tokens_far.1, s32[4,128]{1,0:T(4,128)} %bitcast.3, f32[4,128]{1,0:T(4,128)} %bitcast.4, f32[2,128]{1,0:T(2,128)} %bitcast.5, f32[32,256,128]{2,1,0:T(8,128)} %gate.1, ...), custom_call_target="tpu_custom_call" | custom-call | tf_op jit(solution)/shard_map/pallas_call | solution.py:567
  200.3 2.9 %shard_map.103 = (bf16[1,2048,512]{2,1,0:T(8,128)(2,1)}, bf16[1,2048,512]{2,1,0:T(8,128)(2,1)}, bf16[1,512,2048]{2,1,0:T(8,128)(2,1)}, bf16[128,2048]{1,0:T(8,128)(2,1)}) custom-call(bf16[2,2048,512]{2,1,0:T(8,128)(2,1)S(1)} %get-tuple-element.7.in_mats, bf16[4,512,512]{2,1,0:T(8,128)(2,1)S(1)} %get-tuple-element.8.out_mat, ...), custom_call_target="tpu_custom_call" | custom-call | tf_op jit(solution)/shard_map/pallas_call | solution.py:629

commit v3 on v2

--- a/solution.py
+++ b/solution.py
@@ -92,7 +92,7 @@
     mix_high, mix_low, rows_out, rows_in, side_out, side_in, totals, part_out, part_in,
     load_sem, token_send, token_recv, route_send, route_recv,
     first_send, first_recv, near_send, near_recv, slot_send, slot_recv,
-    second_send, second_recv, back_send, back_recv, side_send, side_recv, part_send, part_recv,
+    second_send, second_recv, back_send, back_recv, side_send, side_recv, part_send, part_recv, ready,
 ):
     n_fs, n_tp, capacity = sizes
     n = n_fs * n_tp
@@ -149,10 +149,13 @@
 
     barrier = pltpu.get_barrier_semaphore()
 
-    def greet(step, carry):
-        to = peer(step)
-        pl.semaphore_signal(barrier, inc=1, device_id=(to[0], to[1]), device_id_type=MESH)
-        return carry
+    across = [device(turn, 0) for turn in range(1, planes)]
+    aside = [device(0, shift) for shift in range(1, n_tp)]
+    along = [device(0, shift * n_tp) for shift in range(1, plane_fs)]
+
+    def greet(semaphore, group):
+        for to in group:
+            pl.semaphore_signal(semaphore, inc=1, device_id=(to[0], to[1]), device_id_type=MESH)
 
     loads = [
         pltpu.make_async_copy(source, target, load_sem.at[i])
@@ -170,7 +173,7 @@
     ]
     for load in loads:
         load.start()
-    lax.fori_loop(0, n - 1, greet, 0)
+    greet(barrier, across + along + aside)
 
     for load in loads[:4]:
         load.wait()
@@ -305,15 +308,19 @@
         lax.fori_loop(start, stop, send_first, 0)
 
     normalize(0, tokens)
-    pl.semaphore_wait(barrier, n - 1)
+    pl.semaphore_wait(barrier, len(across + along + aside))
+    greet(ready.at[0], aside)
     for each in route_copies:
         each.start()
     token_copies[1].start()
     token_copies[0].start()
+    pl.semaphore_wait(ready.at[0], len(aside))
+    greet(ready.at[1], along)
     fill_slots(0, routes_t)
     loads[4].wait()
     loads[5].wait()
     cast_first(0)
+    pl.semaphore_wait(ready.at[1], len(along))
     send_some(0, n // 8)
     send_slots(0)
     send_some(n // 8, 3 * n // 8)
@@ -613,7 +620,8 @@
             dma,
         ]
         + [dma((chunks,))] * 2
-        + [dma((pieces,))] * 6,
+        + [dma((pieces,))] * 6
+        + [pltpu.SemaphoreType.REGULAR((2,))],
         compiler_params=pltpu.CompilerParams(
             collective_id=0, has_side_effects=True, vmem_limit_bytes=52 * 1024 * 1024
         ),

time: 203 us -> 201 us (level); the launches traced: 203 us -> 199 us
  Pallas kernels: 203 us -> 198 us
    pallas_call x1, Pallas kernels: 200 us -> 195 us  [direct_shards(): pl.pallas_call(functools.partial(exchange_kernel, (n_fs, n_tp, capacity))...]
where the time goes in v3:
time: 201 us; the launch traced here: 199 us
  Pallas kernels  198 us (99%)
    pallas_call x1, Pallas kernels, direct_shards(): pl.pallas_call(functools.partial(exchange_kernel, (n_fs, n_tp, capacity))...  195 us

profile of v3, /device:TPU:8, one launch (start us, length us, event | category | flops | bytes accessed | tf_op | source)
XLA Modules:
  0.0 199.0 jit_solution(13452127981150444979)
XLA Ops:
  0.6 195.4 %shard_map.102 = (bf16[2,2048,512]{2,1,0:T(8,128)(2,1)S(1)}, bf16[4,512,512]{2,1,0:T(8,128)(2,1)S(1)}, bf16[128,2048]{1,0:T(8,128)(2,1)S(1)}) custom-call(bf16[128,2048]{1,0:T(8,128)(2,1)} %tokens_far.1, s32[4,128]{1,0:T(4,128)} %bitcast.3, f32[4,128]{1,0:T(4,128)} %bitcast.4, f32[2,128]{1,0:T(2,128)} %bitcast.5, f32[32,256,128]{2,1,0:T(8,128)} %gate.1, ...), custom_call_target="tpu_custom_call" | custom-call | tf_op jit(solution)/shard_map/pallas_call | solution.py:574
  196.0 2.9 %shard_map.103 = (bf16[1,2048,512]{2,1,0:T(8,128)(2,1)}, bf16[1,2048,512]{2,1,0:T(8,128)(2,1)}, bf16[1,512,2048]{2,1,0:T(8,128)(2,1)}, bf16[128,2048]{1,0:T(8,128)(2,1)}) custom-call(bf16[2,2048,512]{2,1,0:T(8,128)(2,1)S(1)} %get-tuple-element.7.in_mats, bf16[4,512,512]{2,1,0:T(8,128)(2,1)S(1)} %get-tuple-element.8.out_mat, ...), custom_call_target="tpu_custom_call" | custom-call | tf_op jit(solution)/shard_map/pallas_call | solution.py:637

commit v4 on v3

--- a/solution.py
+++ b/solution.py
@@ -94,7 +94,7 @@
     first_send, first_recv, near_send, near_recv, slot_send, slot_recv,
     second_send, second_recv, back_send, back_recv, side_send, side_recv, part_send, part_recv, ready,
 ):
-    n_fs, n_tp, capacity = sizes
+    n_fs, n_tp, capacity, splits = sizes
     n = n_fs * n_tp
     fs, tp = lax.axis_index("fs"), lax.axis_index("tp")
     tok_rows, width = tokens.shape
@@ -394,8 +394,17 @@
     def second_all(c):
         return take(out_tiles.at[pl.ds(0, n // 2), c], second_send.at[c], second_recv.at[c])
 
+    bounds = [
+        (c, i * block // parts, (i + 1) * block // parts)
+        for c, parts in enumerate(splits)
+        for i in range(parts)
+    ]
+    pieces = len(bounds)
+
     def back_all(j):
-        return take(rows_in.at[j, pl.ds(0, plane - 1)], back_send.at[j], back_recv.at[j])
+        c, start, stop = bounds[j]
+        rows = rows_in.at[c, pl.ds(0, plane - 1), :, :, start:stop]
+        return take(rows, back_send.at[j], back_recv.at[j])
 
     slots_all.wait_recv()
     first_all.wait_recv()
@@ -418,34 +427,48 @@
     lax.fori_loop(0, active.shape[0], activate, 0)
     near_all.wait_recv()
 
-    pieces, piece = rows_out.shape[0], rows_out.shape[-1]
-    split = pieces // chunks
-
     def back_copy(j, shift):
         to = device(0, shift)
-        return remote(
-            rows_out.at[j, to[2]], rows_in.at[j, spot], back_send.at[j], back_recv.at[j], to
+        c, start, stop = bounds[j]
+        return remote(
+            rows_out.at[c, to[2], :, :, start:stop],
+            rows_in.at[c, spot, :, :, start:stop],
+            back_send.at[j],
+            back_recv.at[j],
+            to,
         )
 
     def side_copy(j):
-        return remote(side_out.at[j], side_in.at[j], side_send.at[j], side_recv.at[j], device(1, 0))
+        c, start, stop = bounds[j]
+        return remote(
+            side_out.at[c, :, :, start:stop],
+            side_in.at[c, :, :, start:stop],
+            side_send.at[j],
+            side_recv.at[j],
+            device(1, 0),
+        )
 
     def part_copy(j):
-        return remote(part_out.at[j], part_in.at[j], part_send.at[j], part_recv.at[j], device(2, 0))
+        c, start, stop = bounds[j]
+        return remote(
+            part_out.at[c, :, start:stop],
+            part_in.at[c, :, start:stop],
+            part_send.at[j],
+            part_recv.at[j],
+            device(2, 0),
+        )
 
     def project(c):
         second_all(c).wait_recv()
-        for i in range(split):
-            j = c * split + i
+        for j in of_chunk(c):
+            cols = slice(*bounds[j][1:])
 
             def project_group(g, carry):
                 rows = jnp.dot(
-                    active[g],
-                    out_mat[c, :, i * piece : (i + 1) * piece],
-                    preferred_element_type=jnp.float32,
+                    active[g], out_mat[c, :, cols], preferred_element_type=jnp.float32
                 )
-                rows_out[j, pl.ds(g * held, held)] = rows.reshape(
-                    held, planes, capacity, piece
+                rows_out[c, pl.ds(g * held, held), :, :, cols] = rows.reshape(
+                    held, planes, capacity, cols.stop - cols.start
                 ).astype(jnp.bfloat16)
                 return carry
 
@@ -456,41 +479,52 @@
                 return carry
 
             lax.fori_loop(1, plane, send_back, 0)
-            rows_in[j, spot] = rows_out[j, spot]
+            rows_in[c, spot, :, :, cols] = rows_out[c, spot, :, :, cols]
 
     span = plane * capacity
 
     def combine(j, turn):
-        rows = rows_in[j, :, turn].astype(jnp.float32).reshape(span, piece).astype(jnp.bfloat16)
+        c, start, stop = bounds[j]
+        rows = rows_in[c, :, turn, :, start:stop].astype(jnp.float32)
+        rows = rows.reshape(span, stop - start).astype(jnp.bfloat16)
         total = jnp.dot(mix_high[turn], rows, preferred_element_type=jnp.float32)
         return total + jnp.dot(mix_low[turn], rows, preferred_element_type=jnp.float32)
 
     def give_side(j):
+        c, start, stop = bounds[j]
         back_all(j).wait_recv()
         for q in range(2):
-            side_out[j, q] = combine(j, 2 * q + 1).astype(jnp.bfloat16)
+            side_out[c, q, :, start:stop] = combine(j, 2 * q + 1).astype(jnp.bfloat16)
         for q in range(1, -1, -1):
-            totals[j, q] = combine(j, 2 * q)
+            totals[c, q, :, start:stop] = combine(j, 2 * q)
             if q == 1:
                 side_copy(j).start()
 
     def give_part(j):
+        c, start, stop = bounds[j]
+        cols = slice(start, stop)
         side_copy(j).wait_recv()
-        part_out[j] = (totals[j, 1] + side_in[j, 1].astype(jnp.float32)).astype(jnp.bfloat16)
-        totals[j, 0] = totals[j, 0] + side_in[j, 0].astype(jnp.float32)
+        part_out[c, :, cols] = (
+            totals[c, 1, :, cols] + side_in[c, 1, :, cols].astype(jnp.float32)
+        ).astype(jnp.bfloat16)
+        totals[c, 0, :, cols] = totals[c, 0, :, cols] + side_in[c, 0, :, cols].astype(jnp.float32)
         part_copy(j).start()
 
     def finish(j):
+        c, start, stop = bounds[j]
         part_copy(j).wait_recv()
-        total = (totals[j, 0] + part_in[j].astype(jnp.float32)).astype(jnp.bfloat16)
-        for k in range(piece // lanes):
-            slab = j % split * (piece // lanes) + k
-            start = slab * down_cols + j // split * lanes
-            mixed[:, start : start + lanes] = total[:, k * lanes : (k + 1) * lanes]
+        total = totals[c, 0, :, start:stop] + part_in[c, :, start:stop].astype(jnp.float32)
+        total = total.astype(jnp.bfloat16)
+        for k in range(start // lanes, stop // lanes):
+            left = k * down_cols + c * lanes
+            mixed[:, left : left + lanes] = total[:, k * lanes - start : (k + 1) * lanes - start]
+
+    def of_chunk(c):
+        return [j for j in range(pieces) if bounds[j][0] == c]
 
     def run(stage, c):
-        for i in range(split):
-            stage(c * split + i)
+        for j in of_chunk(c):
+            stage(j)
 
     for c in range(chunks):
         project(c)
@@ -500,11 +534,13 @@
             send_chunk(c + 2)
         if c > 1:
             run(give_part, c - 2)
-    for i in range(split):
-        give_side((chunks - 1) * split + i)
-        if i == 0:
-            run(give_part, chunks - 2)
-    run(give_part, chunks - 1)
+    last = of_chunk(chunks - 1)
+    give_side(last[0])
+    run(give_part, chunks - 2)
+    for j in last[1:]:
+        give_side(j)
+    for j in last:
+        give_part(j)
     for j in range(pieces):
         finish(j)
 
@@ -563,7 +599,8 @@
     chunks = down_cols // lanes
     block = n_tp * lanes
     plane = n // 4
-    pieces, piece = chunks * 2, block // 2
+    splits = (2,) * chunks
+    pieces = sum(splits)
     per_token = routes.shape[1]
     capacity = max(2, 3 * tok_rows * per_token // (2 * n))
     bf16, f32 = jnp.bfloat16, jnp.float32
@@ -572,7 +609,7 @@
     dma = pltpu.SemaphoreType.DMA
     groups = 4
     in_mats, out_mat, rows = pl.pallas_call(
-        functools.partial(exchange_kernel, (n_fs, n_tp, capacity)),
+        functools.partial(exchange_kernel, (n_fs, n_tp, capacity, splits)),
         out_shape=(
             pltpu.VMEM((2, width, hidden), bf16),
             pltpu.VMEM((chunks, hidden, block), bf16),
@@ -600,13 +637,13 @@
             pltpu.VMEM((3, per_token, tok_rows), f32),
             pltpu.VMEM((4, tok_rows, plane * capacity), bf16),
             pltpu.VMEM((4, tok_rows, plane * capacity), bf16),
-            pltpu.VMEM((pieces, plane, 4, capacity, piece), bf16),
-            pltpu.VMEM((pieces, plane, 4, capacity, piece), bf16),
-            pltpu.VMEM((pieces, 2, tok_rows, piece), bf16),
-            pltpu.VMEM((pieces, 2, tok_rows, piece), bf16),
-            pltpu.VMEM((pieces, 2, tok_rows, piece), f32),
-            pltpu.VMEM((pieces, tok_rows, piece), bf16),
-            pltpu.VMEM((pieces, tok_rows, piece), bf16),
+            pltpu.VMEM((chunks, plane, 4, capacity, block), bf16),
+            pltpu.VMEM((chunks, plane, 4, capacity, block), bf16),
+            pltpu.VMEM((chunks, 2, tok_rows, block), bf16),
+            pltpu.VMEM((chunks, 2, tok_rows, block), bf16),
+            pltpu.VMEM((chunks, 2, tok_rows, block), f32),
+            pltpu.VMEM((chunks, tok_rows, block), bf16),
+            pltpu.VMEM((chunks, tok_rows, block), bf16),
             dma((7,)),
             dma((3,)),
             dma((3,)),

time: 201 us -> 201 us (level)
  no operation moved by 1% of the time
where the time goes in v4:
time: 201 us; the launch traced here: 199 us
  Pallas kernels  198 us (99%)
    pallas_call x1, Pallas kernels, direct_shards(): pl.pallas_call(functools.partial(exchange_kernel, (n_fs, n_tp, capacity,...  196 us

profile of v4, /device:TPU:8, one launch (start us, length us, event | category | flops | bytes accessed | tf_op | source)
XLA Modules:
  0.0 199.1 jit_solution(7010601227769714154)
XLA Ops:
  0.6 195.5 %shard_map.102 = (bf16[2,2048,512]{2,1,0:T(8,128)(2,1)S(1)}, bf16[4,512,512]{2,1,0:T(8,128)(2,1)S(1)}, bf16[128,2048]{1,0:T(8,128)(2,1)S(1)}) custom-call(bf16[128,2048]{1,0:T(8,128)(2,1)} %tokens_far.1, s32[4,128]{1,0:T(4,128)} %bitcast.3, f32[4,128]{1,0:T(4,128)} %bitcast.4, f32[2,128]{1,0:T(2,128)} %bitcast.5, f32[32,256,128]{2,1,0:T(8,128)} %gate.1, ...), custom_call_target="tpu_custom_call" | custom-call | tf_op jit(solution)/shard_map/pallas_call | solution.py:611
  196.2 2.9 %shard_map.103 = (bf16[1,2048,512]{2,1,0:T(8,128)(2,1)}, bf16[1,2048,512]{2,1,0:T(8,128)(2,1)}, bf16[1,512,2048]{2,1,0:T(8,128)(2,1)}, bf16[128,2048]{1,0:T(8,128)(2,1)}) custom-call(bf16[2,2048,512]{2,1,0:T(8,128)(2,1)S(1)} %get-tuple-element.7.in_mats, bf16[4,512,512]{2,1,0:T(8,128)(2,1)S(1)} %get-tuple-element.8.out_mat, ...), custom_call_target="tpu_custom_call" | custom-call | tf_op jit(solution)/shard_map/pallas_call | solution.py:674

commit v5 on v4

--- a/solution.py
+++ b/solution.py
@@ -316,12 +316,12 @@
     token_copies[0].start()
     pl.semaphore_wait(ready.at[0], len(aside))
     greet(ready.at[1], along)
-    fill_slots(0, routes_t)
     loads[4].wait()
     loads[5].wait()
     cast_first(0)
     pl.semaphore_wait(ready.at[1], len(along))
     send_some(0, n // 8)
+    fill_slots(0, routes_t)
     send_slots(0)
     send_some(n // 8, 3 * n // 8)
     for each in route_copies:

time: 201 us -> 201 us (level)
  no operation moved by 1% of the time
where the time goes in v5:
time: 201 us; the launch traced here: 199 us
  Pallas kernels  198 us (99%)
    pallas_call x1, Pallas kernels, direct_shards(): pl.pallas_call(functools.partial(exchange_kernel, (n_fs, n_tp, capacity,...  196 us

profile of v5, /device:TPU:8, one launch (start us, length us, event | category | flops | bytes accessed | tf_op | source)
XLA Modules:
  0.0 199.1 jit_solution(10331273104478528521)
XLA Ops:
  0.6 195.5 %shard_map.102 = (bf16[2,2048,512]{2,1,0:T(8,128)(2,1)S(1)}, bf16[4,512,512]{2,1,0:T(8,128)(2,1)S(1)}, bf16[128,2048]{1,0:T(8,128)(2,1)S(1)}) custom-call(bf16[128,2048]{1,0:T(8,128)(2,1)} %tokens_far.1, s32[4,128]{1,0:T(4,128)} %bitcast.3, f32[4,128]{1,0:T(4,128)} %bitcast.4, f32[2,128]{1,0:T(2,128)} %bitcast.5, f32[32,256,128]{2,1,0:T(8,128)} %gate.1, ...), custom_call_target="tpu_custom_call" | custom-call | tf_op jit(solution)/shard_map/pallas_call | solution.py:611
  196.2 2.9 %shard_map.103 = (bf16[1,2048,512]{2,1,0:T(8,128)(2,1)}, bf16[1,2048,512]{2,1,0:T(8,128)(2,1)}, bf16[1,512,2048]{2,1,0:T(8,128)(2,1)}, bf16[128,2048]{1,0:T(8,128)(2,1)}) custom-call(bf16[2,2048,512]{2,1,0:T(8,128)(2,1)S(1)} %get-tuple-element.7.in_mats, bf16[4,512,512]{2,1,0:T(8,128)(2,1)S(1)} %get-tuple-element.8.out_mat, ...), custom_call_target="tpu_custom_call" | custom-call | tf_op jit(solution)/shard_map/pallas_call | solution.py:674
